TPU v7x, 512 devices: a whole 4x4x16 slice. The times are simulated.
512 devices in a mesh: sp: 64 (over z, y), tp: 8 (over x, core).
Axes of the slice: x: 4, y: 4, z: 16, core: 2. Of those that a mesh axis runs over, the one named last changes fastest.
Arguments:
- residual: bfloat16 [8192, 2048], P('sp'), may hold values from -6 to 6
- query_first: bfloat16 [8192, 8, 128], P('sp', 'tp'), may hold values from -6.5 to 6.5
- key_first: bfloat16 [8192, 8, 128], P('sp', 'tp'), may hold values from -6.5 to 6.5
- value_first: bfloat16 [8192, 8, 128], P('sp', 'tp'), may hold values from -6 to 6
- query_second: bfloat16 [8192, 8, 64], P('sp', 'tp'), may hold values from -6.5 to 6.5
- key_second: bfloat16 [8192, 8, 64], P('sp', 'tp'), may hold values from -6.5 to 6.5
- value_second: bfloat16 [8192, 8, 64], P('sp', 'tp'), may hold values from -6 to 6
- balance_first: float32 [8], P('tp'), may hold values from 0.3 to 0.8
- balance_second: float32 [8], P('tp'), may hold values from 0.3 to 0.8
- head_gain_first: float32 [128], replicated, may hold values from 0.1 to 1.9
- head_gain_second: float32 [64], replicated, may hold values from 0.1 to 1.9
- out_first: bfloat16 [1024, 2048], P('tp'), may hold values from -0.15625 to 0.15625
- out_second: bfloat16 [512, 2048], P('tp'), may hold values from -0.15625 to 0.15625
- mlp_gain: float32 [2048], replicated, may hold values from 0.1 to 1.9
- up_weight: bfloat16 [2048, 8192], P('sp', 'tp'), may hold values from -0.125 to 0.125
- down_weight: bfloat16 [2048, 8192], P('sp', 'tp'), may hold values from -0.0625 to 0.0625
Outputs:
- layer_out: bfloat16 [8192, 2048], P('sp')
All inputs are finite; a program needn't handle non-finite values.
Results may differ from a plain program's by a relative error of at most 0.018.
Values may be sent and summed in bfloat16 or wider, within the bound.
A program may use at most 64 MiB of HBM per device.

v0:
```python
import math

import jax
import jax.numpy as jnp
from jax import lax
from jax.sharding import PartitionSpec as P

DK_A = 64
DK_B = 32


EPSILON = 1e-06
HEAD_SCALE = 0.8


def side_by_side(arrays, axis, dim, along):
    ends, at = ([], 0)
    for a in arrays[:-1]:
        at += a.shape[along]
        ends.append(at)
    both = jnp.concatenate(arrays, axis=along)
    return tuple(jnp.split(lax.all_gather(both, axis, axis=dim, tiled=True), ends, axis=along))


def copy_for_each(value, axis):
    length = lax.axis_size(axis)
    return lax.all_to_all(
        jnp.broadcast_to(value[None], (length, *value.shape)), axis, 0, 0, tiled=True
    )


def of_everyone(value, axis):
    everything = copy_for_each(value, axis)
    return jnp.sum(everything.astype(jnp.float32), axis=0)


def over_pieces(value, axis):
    tiles = lax.all_gather(value, axis).astype(jnp.float32)
    return tiles.sum(axis=0)


def attend(queries, keys, values, balance, gain, device, head_size):
    tokens = queries.shape[0]
    heads = queries.shape[1]
    seq = keys.shape[0]
    depth = values.shape[2]
    block = math.gcd(512, seq)
    scale = head_size ** (-0.5)
    query_maps = queries.reshape(tokens, heads, 2, head_size)
    key_maps = keys.reshape(seq, heads, 2, head_size)
    first_row = device * tokens
    positions = first_row + jnp.arange(tokens, dtype=jnp.int32)
    needed = (first_row + tokens + block - 1) // block

    def block_scores(number):
        start = number * block
        key_block = lax.dynamic_slice_in_dim(key_maps, start, block, 0)
        scores = (
            jnp.einsum("qhmd,khmd->hmqk", query_maps, key_block, preferred_element_type=jnp.float32)
            * scale
        )
        columns = start + jnp.arange(block, dtype=jnp.int32)
        visible = columns[None, :] <= positions[:, None]
        return (jnp.where(visible, scores, -jnp.inf), start)

    def statistics(number, carry):
        highest, total = carry
        scores, start = block_scores(number)
        fresh = jnp.maximum(highest, jnp.max(scores, axis=-1, keepdims=True))
        total = total * jnp.exp(highest - fresh) + jnp.sum(
            jnp.exp(scores - fresh), axis=-1, keepdims=True
        )
        return (fresh, total)

    start_high = jnp.full((heads, 2, tokens, 1), -jnp.inf, jnp.float32)
    start_total = jnp.zeros((heads, 2, tokens, 1), jnp.float32)
    highest, total = lax.fori_loop(0, needed, statistics, (start_high, start_total))

    def accumulate(number, result):
        scores, start = block_scores(number)
        probs = jnp.exp(scores - highest) / total
        mixed = (probs[:, 0] - balance[:, None, None] * probs[:, 1]).astype(jnp.bfloat16)
        value_block = lax.dynamic_slice_in_dim(values, start, block, 0)
        return result + jnp.einsum(
            "hqk,khe->qhe", mixed, value_block, preferred_element_type=jnp.float32
        )

    summed = lax.fori_loop(0, needed, accumulate, jnp.zeros((tokens, heads, depth), jnp.float32))
    power = jnp.mean(summed * summed, axis=-1, keepdims=True)
    normed = summed * lax.rsqrt(power + EPSILON) * gain * HEAD_SCALE
    return normed.astype(jnp.bfloat16).reshape(tokens, heads * depth)


def body(
    residual,
    query_first,
    key_first,
    value_first,
    query_second,
    key_second,
    value_second,
    balance_first,
    balance_second,
    head_gain_first,
    head_gain_second,
    out_first,
    out_second,
    mlp_gain,
    up_weight,
    down_weight,
):
    device = lax.axis_index("sp")
    keys_first, values_first, keys_second, values_second, up_whole, down_whole = (
        *side_by_side((key_first, value_first, key_second, value_second), "sp", 0, 2),
        *side_by_side((up_weight, down_weight), "sp", 0, 1),
    )
    heads_first = attend(
        query_first, keys_first, values_first, balance_first, head_gain_first, device, DK_A
    )
    heads_second = attend(
        query_second, keys_second, values_second, balance_second, head_gain_second, device, DK_B
    )
    head_term = jnp.dot(heads_first, out_first, preferred_element_type=jnp.float32) + jnp.dot(
        heads_second, out_second, preferred_element_type=jnp.float32
    )
    head_total = of_everyone(head_term.astype(jnp.bfloat16), "tp").astype(jnp.float32)
    mixed = (residual.astype(jnp.float32) + head_total).astype(jnp.bfloat16)
    mixed_float = mixed.astype(jnp.float32)
    power = jnp.mean(mixed_float * mixed_float, axis=-1, keepdims=True)
    normed = (mixed_float * lax.rsqrt(power + EPSILON) * mlp_gain).astype(jnp.bfloat16)
    lifted = jnp.dot(normed, up_whole, preferred_element_type=jnp.float32)
    active = jax.nn.relu(lifted)
    hidden = (active * active).astype(jnp.bfloat16)
    down_term = lax.dot_general(
        hidden, down_whole, (((1,), (1,)), ((), ())), preferred_element_type=jnp.float32
    )
    added = over_pieces(down_term.astype(jnp.bfloat16), "tp").astype(jnp.float32)
    return (mixed_float + added).astype(jnp.bfloat16)


def solution(mesh):
    in_specs = (
        P("sp", None),
        P("sp", "tp", None),
        P("sp", "tp", None),
        P("sp", "tp", None),
        P("sp", "tp", None),
        P("sp", "tp", None),
        P("sp", "tp", None),
        P("tp"),
        P("tp"),
        P(),
        P(),
        P("tp", None),
        P("tp", None),
        P(),
        P("sp", "tp"),
        P("sp", "tp"),
    )
    out_specs = P("sp", None)
    return jax.shard_map(body, mesh=mesh, in_specs=in_specs, out_specs=out_specs, check_vma=False)
```

profile of v0, /device:TPU:1, one launch (start us, length us, event | category | flops | bytes accessed | tf_op | source)
XLA Modules:
  0.0 377.8 jit_solution(1925370097816546670)
XLA Ops:
  6.5 0.9 copy.29
  7.5 0.9 copy.30
  8.4 1.4 pad_maximum_fusion.1
  9.8 1.5 pad_maximum_fusion
  11.4 0.9 copy.31
  12.3 149.7 %all-gather.5.cloned.1.call-done = bf16[8192,1,384]{0,2,1:T(8,128)(2,1)} async-done(((bf16[128,1,384]{0,2,1:T(8,128)(2,1)}), bf16[8192,1,384]{0,2,1:T(8,128)(2,1)}) %all-gather.5.cloned.1.call-update) | async-done | bytes 6291472 | tf_op jit(solution)/shard_map/all_gather | solution.py:22
  162.0 1.7 fusion.104
  163.8 0.6 while.50
  163.8 0.1 broadcast_compare_fusion.10
  163.9 0.3 fusion.129
  164.4 1.3 while.51
  164.5 0.1 broadcast_compare_fusion.11
  164.6 0.3 fusion.134
  164.9 0.8 fusion.135
  165.8 3.9 %fusion.105 = (bf16[8192,1,128]{0,2,1:T(8,128)(2,1)S(1)}, bf16[8192,1,128]{0,2,1:T(8,128)(2,1)}) fusion(bf16[8192,1,384]{0,2,1:T(8,128)(2,1)} %all-gather.5.cloned.1.call-done), kind=kLoop, calls=%fused_computation.125 | loop fusion | bytes 8388608 | tf_op jit(solution)/shard_map/split | solution.py:22
  169.7 0.6 while.48
  169.9 0.3 fusion.122
  170.4 2.3 while.49
  170.5 0.3 fusion.127
  170.9 1.7 fusion.128
  172.7 0.4 fusion.89
  173.1 0.4 fusion.62
  173.5 0.5 broadcast_in_dim.68
  174.1 62.9 %all_to_all.5 = bf16[8,128,2048]{2,1,0:T(8,128)(2,1)S(1)} all-to-all(bf16[8,128,2048]{2,1,0:T(8,128)(2,1)S(1)} %broadcast_in_dim.68), channel_id=1, replica_groups=mesh['sp'=64,'tp'=8] {'tp'}, dimensions={0} | all-to-all | bytes 8388608 | tf_op jit(solution)/shard_map/all_to_all | solution.py:27
  237.0 0.7 convert_reduce_fusion.1
  237.7 0.3 copy-done.1
  238.0 0.2 fusion.77
  238.3 79.8 %all-gather.7.cloned.1.call-done = bf16[2048,2048]{1,0:T(8,128)(2,1)} async-done(((bf16[32,2048]{1,0:T(8,128)(2,1)}), bf16[2048,2048]{1,0:T(8,128)(2,1)}) %all-gather.7.cloned.1.call-update) | async-done | bytes 8388624 | tf_op jit(solution)/shard_map/all_gather | solution.py:22
  318.1 6.4 %fusion.63 = bf16[128,2048]{1,0:T(8,128)(2,1)} fusion(bf16[2048,2048]{1,0:T(8,128)(2,1)} %all-gather.7.cloned.1.call-done, bf16[128,2048]{1,0:T(8,128)(2,1)S(1)} %get-tuple-element.385, f32[2048]{0:T(1024)S(1)} %copy-done.6, f32[128]{0:T(128)S(1)} %add_rsqrt_fusion), kind=kOutput, calls=%fused_computation.86 | convolution fusion | flops 1075445760 | bytes 9445888 | tf_op jit(solution)/shard_map/dot_general | solution.py:134
  324.5 42.9 %all-gather.9.cloned.1.call-done = bf16[1024,2048]{1,0:T(8,128)(2,1)} async-done(((bf16[128,2048]{1,0:T(8,128)(2,1)}), bf16[1024,2048]{1,0:T(8,128)(2,1)}) %all-gather.9.cloned.1.call-update) | async-done | bytes 4194320 | tf_op jit(solution)/shard_map/all_gather | solution.py:38
  367.4 3.0 convert_reduce_fusion
  370.4 0.9 fusion.80
  (48 shorter events, 0.8 us)
Async XLA Ops:
  6.5 166.2 %copy-start = (bf16[128,2048]{1,0:T(8,128)(2,1)S(1)}, bf16[128,2048]{1,0:T(8,128)(2,1)}, u32[]{:S(2)}) copy-start(bf16[128,2048]{1,0:T(8,128)(2,1)} %param.35) | copy-start | bytes 1572868
  6.5 157.2 %copy-start.5 = (bf16[128,1,64]{0,2,1:T(8,128)(2,1)S(1)}, bf16[128,1,64]{0,2,1:T(8,128)(2,1)}, u32[]{:S(2)}) copy-start(bf16[128,1,64]{0,2,1:T(8,128)(2,1)} %param.28) | copy-start | bytes 49156
  6.5 155.5 %all-gather.5.cloned.1.call-start = ((), (), s32[]{:S(2)}) async-start(), calls=%async_computation.1 | async-start | bytes 6389760 | tf_op jit(solution)/shard_map/all_gather | solution.py:22
  9.8 308.3 %all-gather.7.cloned.1.call-start = ((), (), s32[]{:S(2)}) async-start(), calls=%async_computation.2 | async-start | bytes 8519680 | tf_op jit(solution)/shard_map/all_gather | solution.py:22
  11.4 356.0 %all-gather.9.cloned.1.call-start = ((), (), s32[]{:S(2)}) async-start(), calls=%async_computation.3 | async-start | bytes 4718592 | tf_op jit(solution)/shard_map/all_gather | solution.py:38
  170.3 2.4 copy-start.3
  170.3 2.8 copy-start.2
  170.3 2.8 copy-start.4
  237.0 1.0 copy-start.1
  237.0 81.1 %copy-start.6 = (f32[2048]{0:T(1024)S(1)}, f32[2048]{0:T(1024)}, u32[]{:S(2)}) copy-start(f32[2048]{0:T(1024)} %param.37) | copy-start | bytes 24580
Sparse Core Ops, SparseCore 0:
  10.2 151.7 all-gather.4
  165.0 153.0 all-gather.6
  324.6 42.7 all-gather.8
where the time goes:
time: 379 us; the launch traced here: 378 us
  waiting for transfers between devices  272 us (72%)
  blocking collectives  62.9 us (17%)
  between operations  13.3 us (4%)
  matrix products  11 us (3%)
  local copies, waits for them, and re-layouts  9.17 us (2%)
  other arithmetic  8.65 us (2%)
    all_gather x2, waiting for transfers between devices, side_by_side(): lax.all_gather(both, axis, axis=dim, tiled=True)  230 us
    all_to_all x1, blocking collectives, copy_for_each(): lax.all_to_all(jnp.broadcast_to(value[None], (length, *value.shape)), axi...  62.9 us
    all_gather x1, waiting for transfers between devices, over_pieces(): tiles = lax.all_gather(value, axis).astype(jnp.float32)  42.9 us
  transfers between devices with their start and end apart: 3, of which 3 were waited for; matrix products, arithmetic and copies ran while one was open for 4% of the time, Pallas kernels for 0%

commit v1 on v0

v1 whole, which is shorter than its diff:
```python
import functools
import math

import jax
import jax.numpy as jnp
from jax import lax
from jax.experimental import pallas as pl
from jax.experimental.pallas import tpu as pltpu
from jax.sharding import PartitionSpec as P

MESH = pl.DeviceIdType.MESH
DK_A = 64
DK_B = 32
EPSILON = 1e-06
HEAD_SCALE = 0.8
NY = 4
NX = 4
ROWS = 128
BLOCK = NY * ROWS
D = 2048
FB = 256
NB = D // FB
LOW = -1e30
RATES = tuple(k**-0.5 * math.log2(math.e) for k in (DK_A, DK_A, DK_B, DK_B))
SPANS = ((0, 128), (128, 256), (256, 320), (320, 384))
F32 = jnp.float32
BF16 = jnp.bfloat16


def nt(a, b):
    return lax.dot_general(a, b, (((1,), (1,)), ((), ())), preferred_element_type=F32)


def kernel(
    nz,
    qkv,
    balances,
    gains,
    mlp_gain,
    residual,
    out_first,
    out_second,
    up,
    down,
    out,
    qbuf,
    qpad,
    kv,
    acc,
    stats,
    xsnd,
    xacc,
    xstats,
    hx,
    hmat,
    wo,
    res,
    wup,
    wdn,
    pb,
    rb,
    mx,
    gb,
    db,
    rd,
    sb,
    rs,
    loc,
    qs,
    qr,
    ks,
    kr,
    ys,
    yr,
    ws,
    wr,
    vs,
    vr,
    os,
    orr,
    xs,
    xr,
    hs,
    hr,
    ps,
    pr,
    dsm,
    drm,
    ss,
    sr,
    fs,
    fr,
    gs,
    gr,
):
    sp = lax.axis_index("sp")
    tp = lax.axis_index("tp")
    z, y = sp // NY, sp % NY
    x, c = tp // 2, tp % 2

    def near(dy, dx):
        return (z * NY + (y + dy) % NY, ((x + dx) % NX) * 2 + c)

    partner = (sp, x * 2 + (1 - c))
    above = (((z + 1) % nz) * NY + y, tp)
    below = (((z + nz - 1) % nz) * NY + y, tp)
    others = [(dy, dx) for dy in range(NY) for dx in range(NX) if dy or dx]

    def send(src, dst, ssem, rsem, device):
        return pltpu.make_async_remote_copy(
            src_ref=src,
            dst_ref=dst,
            send_sem=ssem,
            recv_sem=rsem,
            device_id=device,
            device_id_type=MESH,
        )

    def arrive(ref, ssem, rsem):
        send(ref, ref, ssem, rsem, partner).wait_recv()

    def left(ref, ssem, rsem):
        send(ref, ref, ssem, rsem, partner).wait_send()

    barrier = pltpu.get_barrier_semaphore()
    for device in [near(dy, dx) for dy, dx in others] + [partner, above, below]:
        pl.semaphore_signal(barrier, inc=1, device_id=device, device_id_type=MESH)

    kv[z, 0] = qkv[2]
    kv[z, 1] = qkv[3].astype(F32).T.astype(BF16)
    kv[z, 2] = qkv[4]
    qbuf[y, 0] = qkv[0]
    qbuf[y, 1] = qkv[1]
    pl.semaphore_wait(barrier, len(others) + 3)

    for ch in range(3):
        for way, device in ((0, above), (1, below)):
            send(
                kv.at[z, ch], kv.at[z, ch], ks.at[way, 0, ch], kr.at[way, 0, ch], device
            ).start()
    for d in range(1, NY):
        send(qkv.at[pl.ds(0, 2)], qbuf.at[y], qs.at[d - 1], qr.at[d - 1], near(d, 0)).start()

    own = pl.ds(pl.multiple_of(z * ROWS + y * 32, 32), 32)
    mine = pl.ds(pl.multiple_of(y * FB, FB), FB)
    tok = pl.ds(pl.multiple_of(y * ROWS, ROWS), ROWS)
    ra = pl.ds(pl.multiple_of(x * 128, 128), 128)
    rbw = pl.ds(pl.multiple_of(512 + x * 64, 64), 64)
    locals_ = [
        pltpu.make_async_copy(up.at[:, mine], wup.at[own], loc.at[0]),
        pltpu.make_async_copy(down.at[:, mine], wdn.at[own], loc.at[1]),
        pltpu.make_async_copy(residual, res.at[tok], loc.at[2]),
        pltpu.make_async_copy(out_first, wo.at[ra], loc.at[3]),
        pltpu.make_async_copy(out_second, wo.at[rbw], loc.at[4]),
    ]
    for copy in locals_:
        copy.start()
    for d in range(1, NY):
        part = pl.ds(pl.multiple_of(((y + d) % NY) * FB, FB), FB)
        send(up.at[:, part], wup.at[own], ys.at[d - 1, 0], yr.at[d - 1, 0], near(d, 0)).start()
        send(down.at[:, part], wdn.at[own], ys.at[d - 1, 1], yr.at[d - 1, 1], near(d, 0)).start()
    for d in range(1, NX):
        send(out_first, wo.at[ra], os.at[d - 1, 0], orr.at[d - 1, 0], near(0, d)).start()
        send(out_second, wo.at[rbw], os.at[d - 1, 1], orr.at[d - 1, 1], near(0, d)).start()
    for d in range(1, NY):
        send(residual, res.at[tok], vs.at[d - 1], vr.at[d - 1], near(d, 0)).start()

    stats[pl.ds(0, 4)] = jnp.full((4, BLOCK), LOW, F32)
    stats[pl.ds(4, 4)] = jnp.zeros((4, BLOCK), F32)
    acc[...] = jnp.zeros_like(acc)

    for d in range(1, NY):
        arrive(qbuf.at[(y + NY - d) % NY], qs.at[d - 1], qr.at[d - 1])
    lane = lax.broadcasted_iota(jnp.int32, (ROWS, 128), 1)
    bounds = ((0, 0, 64), (0, 64, 128), (1, 0, 32), (1, 32, 64))
    for i, (g, low, high) in enumerate(bounds):
        keep = ((lane >= low) & (lane < high)).astype(F32).astype(BF16)
        for j in range(NY):
            qpad[i, pl.ds(j * ROWS, ROWS)] = qbuf[j, g] * keep

    def attend(slot, masked):
        both = kv[slot, 2].astype(F32).T.astype(BF16)
        for i in range(4):
            keys = kv[slot, 0] if i < 2 else kv[slot, 2]
            values = kv[slot, 1] if i < 2 else both[64:128]
            lo, hi = SPANS[i]
            for half in range(2):
                cols = pl.ds(half * 256, 256)
                s = nt(keys, qpad[i, cols])
                if masked:
                    kpos = y * ROWS + lax.broadcasted_iota(jnp.int32, s.shape, 0)
                    qpos = half * 256 + lax.broadcasted_iota(jnp.int32, s.shape, 1)
                    visible = kpos <= qpos
                    s = jnp.where(visible, s, LOW)
                old = stats[pl.ds(i, 1), cols]
                new = jnp.maximum(old, jnp.max(s, axis=0, keepdims=True))
                p = jnp.exp2((s - new) * RATES[i])
                if masked:
                    p = jnp.where(visible, p, 0.0)
                alpha = jnp.exp2((old - new) * RATES[i])
                stats[pl.ds(i, 1), cols] = new
                stats[pl.ds(4 + i, 1), cols] = stats[pl.ds(4 + i, 1), cols] * alpha + jnp.sum(
                    p, axis=0, keepdims=True
                )
                rows = pl.ds(lo, hi - lo)
                acc[rows, cols] = acc[rows, cols] * alpha + jnp.dot(
                    values, p.astype(BF16), preferred_element_type=F32
                )

    attend(z, True)

    def ring(k, _):
        upper = lax.rem(z - (k + 1) + nz, nz)
        lower = lax.rem(z + k + 1, nz)
        for ch in range(3):
            arrive(kv.at[upper, ch], ks.at[0, k, ch], kr.at[0, k, ch])

            @pl.when(k < nz // 2 - 1)
            def _():
                ref = kv.at[upper, ch]
                send(ref, ref, ks.at[0, k + 1, ch], kr.at[0, k + 1, ch], above).start()
                arrive(kv.at[lower, ch], ks.at[1, k, ch], kr.at[1, k, ch])

            @pl.when(k < nz // 2 - 2)
            def _():
                ref = kv.at[lower, ch]
                send(ref, ref, ks.at[1, k + 1, ch], kr.at[1, k + 1, ch], below).start()

        def side(way, _):
            slot = jnp.where(way == 0, upper, lower)
            first = (way == 0) & (k + 1 <= z)
            second = (way == 1) & (z + k + 1 >= nz) & (k < nz // 2 - 1)

            @pl.when(first | second)
            def _():
                attend(slot, False)

            return 0

        lax.fori_loop(0, 2, side, 0)
        return 0

    lax.fori_loop(0, nz // 2, ring, 0)

    def shard(ref, at):
        return ref.at[pl.ds(pl.multiple_of(at * ROWS, ROWS), ROWS)]

    for copy in locals_:
        copy.wait()
    for d in range(1, NY):
        rows = pl.ds(pl.multiple_of(z * ROWS + ((y + NY - d) % NY) * 32, 32), 32)
        for i, w in enumerate((wup, wdn)):
            arrive(w.at[rows], ys.at[d - 1, i], yr.at[d - 1, i])
    for i, w in enumerate((wup, wdn)):
        for way, device in ((0, above), (1, below)):
            send(shard(w, z), shard(w, z), ws.at[way, 0, i], wr.at[way, 0, i], device).start()

    def turn(k):
        upper = lax.rem(z - (k + 1) + nz, nz)
        lower = lax.rem(z + k + 1, nz)
        for i, w in enumerate((wup, wdn)):
            ref = shard(w, upper)
            arrive(ref, ws.at[0, k, i], wr.at[0, k, i])
            if k < nz // 2 - 1:
                send(ref, ref, ws.at[0, k + 1, i], wr.at[0, k + 1, i], above).start()
                ref = shard(w, lower)
                arrive(ref, ws.at[1, k, i], wr.at[1, k, i])
                if k < nz // 2 - 2:
                    send(ref, ref, ws.at[1, k + 1, i], wr.at[1, k + 1, i], below).start()

    turns = list(range(nz // 2))

    def turn_some(count):
        for k in turns[:count]:
            turn(k)
        del turns[:count]

    turn_some(0)
    for j in range(NY):
        xsnd[j] = acc[:, pl.ds(j * ROWS, ROWS)].astype(BF16)
    for d in range(1, NY):
        there = (y + d) % NY
        part = stats.at[:, pl.ds(pl.multiple_of(there * ROWS, ROWS), ROWS)]
        send(xsnd.at[there], xacc.at[y], xs.at[d - 1, 0], xr.at[d - 1, 0], near(d, 0)).start()
        send(part, xstats.at[y], xs.at[d - 1, 1], xr.at[d - 1, 1], near(d, 0)).start()
    xacc[y] = xsnd[y]
    xstats[y] = stats[:, tok]
    turn_some(1)
    for d in range(1, NY):
        there = (y + NY - d) % NY
        arrive(xacc.at[there], xs.at[d - 1, 0], xr.at[d - 1, 0])
        arrive(xstats.at[there], xs.at[d - 1, 1], xr.at[d - 1, 1])

    maps = []
    for i in range(4):
        lo, hi = SPANS[i]
        tops = [xstats[j, i : i + 1] for j in range(NY)]
        top = functools.reduce(jnp.maximum, tops)
        shares = [jnp.exp2((t - top) * RATES[i]) for t in tops]
        total = sum(w * xstats[j, 4 + i : 5 + i] for j, w in enumerate(shares))
        maps.append(
            sum(
                xacc[j, pl.ds(lo, hi - lo)].astype(F32) * (w / total)
                for j, w in enumerate(shares)
            )
        )
    for g in range(2):
        mixed = maps[2 * g] - balances[g] * maps[2 * g + 1]
        size = mixed.shape[0]
        power = jnp.mean(mixed * mixed, axis=0, keepdims=True)
        gain = jnp.broadcast_to(gains[g : g + 1], (128, 128)).T[0:size]
        normed = mixed * lax.rsqrt(power + EPSILON) * gain * HEAD_SCALE
        hx[y, x, pl.ds(128 * g, size)] = normed.astype(BF16)
    for n, (dy, dx) in enumerate(others):
        send(hx.at[y, x], hx.at[y, x], hs.at[n], hr.at[n], near(dy, dx)).start()
    turn_some(3)
    for d in range(1, NX):
        there = (x + NX - d) % NX
        for i, (size, base) in enumerate(((128, 0), (64, 512))):
            ref = wo.at[pl.ds(pl.multiple_of(base + there * size, size), size)]
            arrive(ref, os.at[d - 1, i], orr.at[d - 1, i])
    for n, (dy, dx) in enumerate(others):
        ref = hx.at[(y + NY - dy) % NY, (x + NX - dx) % NX]
        arrive(ref, hs.at[n], hr.at[n])
    for j in range(NY):
        rows = pl.ds(j * ROWS, ROWS)
        for i in range(NX):
            hmat[rows, pl.ds(i * 128, 128)] = hx[j, i, pl.ds(0, 128)].astype(F32).T.astype(BF16)
        for i in range(NX // 2):
            pair = jnp.concatenate(
                [hx[j, 2 * i, pl.ds(128, 64)], hx[j, 2 * i + 1, pl.ds(128, 64)]], axis=0
            )
            hmat[rows, pl.ds(512 + i * 128, 128)] = pair.astype(F32).T.astype(BF16)

    def block(n):
        return pl.ds(pl.multiple_of(n * FB, FB), FB)

    def project(n, _):
        pb[n] = jnp.dot(hmat[...], wo[:, block(n)], preferred_element_type=F32).astype(BF16)
        send(pb.at[n], rb.at[n], ps.at[n], pr.at[n], partner).start()
        return 0

    lax.fori_loop(0, NB, project, 0)
    for d in range(1, NY):
        there = pl.ds(pl.multiple_of(((y + NY - d) % NY) * ROWS, ROWS), ROWS)
        arrive(res.at[there], vs.at[d - 1], vr.at[d - 1])
    turn_some(2)

    def mix(n, power):
        arrive(rb.at[n], ps.at[n], pr.at[n])
        cols = block(n)
        mixed = (
            res[:, cols].astype(F32) + (pb[n].astype(F32) + rb[n].astype(F32))
        ).astype(BF16)
        mx[:, cols] = mixed
        wide = mixed.astype(F32)
        gb[:, cols] = (wide * mlp_gain[:, cols]).astype(BF16)
        square = wide * wide
        return power + (square[:, 0:128] + square[:, 128:256])

    power = lax.fori_loop(0, NB, mix, jnp.zeros((BLOCK, 128), F32))
    scale = lax.rsqrt(jnp.sum(power, axis=-1, keepdims=True) * (1.0 / D) + EPSILON)
    turn_some(len(turns))
    lifted = jnp.dot(gb[...], wup[...], preferred_element_type=F32) * scale
    active = jnp.maximum(lifted, 0.0)
    gb[:, pl.ds(0, FB)] = (active * active).astype(BF16)

    def lower_part(n, _):
        rows = pl.ds(pl.multiple_of(n * FB, FB), FB)
        term = nt(gb[:, pl.ds(0, FB)], wdn[rows]).astype(BF16)
        for j in range(NY):
            for h in range(2):
                at = j * ROWS + h * 64
                db[n, h, pl.ds(j * 64, 64)] = term[at : at + 64]
        send(db.at[n, 1 - c], rd.at[n], dsm.at[n], drm.at[n], partner).start()
        return 0

    lax.fori_loop(0, NB, lower_part, 0)

    def gather(n, _):
        arrive(rd.at[n], dsm.at[n], drm.at[n])
        both = (db[n, c].astype(F32) + rd[n].astype(F32)).astype(BF16)
        cols = block(n)
        for j in range(16):
            sb[j, :, cols] = both[j * 16 : j * 16 + 16]
        return 0

    lax.fori_loop(0, NB, gather, 0)
    for n, (dy, dx) in enumerate(others):
        to = ((y + dy) % NY) * NX + (x + dx) % NX
        send(sb.at[to], rs.at[y * NX + x], ss.at[n], sr.at[n], near(dy, dx)).start()
    rs[y * NX + x] = sb[y * NX + x]
    for n, (dy, dx) in enumerate(others):
        ref = rs.at[((y + NY - dy) % NY) * NX + (x + NX - dx) % NX]
        arrive(ref, ss.at[n], sr.at[n])

    def final(n, _):
        cols = block(n)
        added = rs[:, :, cols].astype(F32).sum(axis=0)
        base = mx[pl.ds(pl.multiple_of(y * ROWS + c * 64 + x * 16, 16), 16), cols].astype(F32)
        out[pl.ds(pl.multiple_of(c * 64 + x * 16, 16), 16), cols] = (base + added).astype(BF16)
        return 0

    lax.fori_loop(0, NB, final, 0)

    def piece(core, at):
        return out.at[pl.ds(pl.multiple_of(core * 64 + at * 16, 16), 16)]

    send(piece(c, x), piece(c, x), gs.at[0], gr.at[0], partner).start()
    for d in range(1, NX):
        send(piece(c, x), piece(c, x), fs.at[d - 1], fr.at[d - 1], near(0, d)).start()
    for d in range(1, NX):
        ref = piece(c, (x + NX - d) % NX)
        arrive(ref, fs.at[d - 1], fr.at[d - 1])
        send(ref, ref, gs.at[d], gr.at[d], partner).start()
    for d in range(NX):
        arrive(piece(1 - c, (x + NX - d) % NX), gs.at[d], gr.at[d])

    for d in range(NX - 1):
        left(piece(c, x), fs.at[d], fr.at[d])
        left(out_first, os.at[d, 0], orr.at[d, 0])
        left(out_second, os.at[d, 1], orr.at[d, 1])
    for d in range(NX):
        left(piece(c, x), gs.at[d], gr.at[d])
    for d in range(NY - 1):
        left(qbuf.at[0], qs.at[d], qr.at[d])
        left(up.at[:, mine], ys.at[d, 0], yr.at[d, 0])
        left(down.at[:, mine], ys.at[d, 1], yr.at[d, 1])
        left(residual, vs.at[d], vr.at[d])
        left(xsnd.at[0], xs.at[d, 0], xr.at[d, 0])
        left(xstats.at[0], xs.at[d, 1], xr.at[d, 1])
    for n in range(len(others)):
        left(hx.at[0, 0], hs.at[n], hr.at[n])
        left(sb.at[0], ss.at[n], sr.at[n])
    for n in range(NB):
        left(pb.at[0], ps.at[n], pr.at[n])
        left(rd.at[0], dsm.at[n], drm.at[n])
    for way, steps in ((0, nz // 2), (1, nz // 2 - 1)):
        for k in range(steps):
            for ch in range(3):
                left(kv.at[0, ch], ks.at[way, k, ch], kr.at[way, k, ch])
            for i in range(2):
                left(shard(wup, 0), ws.at[way, k, i], wr.at[way, k, i])


def layer(
    residual,
    query_first,
    key_first,
    value_first,
    query_second,
    key_second,
    value_second,
    balance_first,
    balance_second,
    head_gain_first,
    head_gain_second,
    out_first,
    out_second,
    mlp_gain,
    up_weight,
    down_weight,
):
    nz = lax.axis_size("sp") // NY
    flat = lambda a: a.reshape(a.shape[0], a.shape[2])
    query_low, key_low, value_low = flat(query_second), flat(key_second), flat(value_second)
    qkv = jnp.stack(
        [
            flat(query_first),
            jnp.concatenate([query_low, jnp.zeros_like(query_low)], axis=1),
            flat(key_first),
            flat(value_first),
            jnp.concatenate([key_low, value_low], axis=1),
        ]
    )
    balances = jnp.concatenate([balance_first, balance_second])
    gains = jnp.stack([head_gain_first, jnp.concatenate([head_gain_second, head_gain_second])])
    vmem = pl.BlockSpec(memory_space=pltpu.VMEM)
    smem = pl.BlockSpec(memory_space=pltpu.SMEM)
    anywhere = pl.BlockSpec(memory_space=pl.ANY)
    half = nz // 2
    dma = lambda *shape: pltpu.SemaphoreType.DMA(shape)
    return pl.pallas_call(
        functools.partial(kernel, nz),
        out_shape=jax.ShapeDtypeStruct((ROWS, D), BF16),
        in_specs=[vmem, smem, vmem, vmem] + [anywhere] * 5,
        out_specs=vmem,
        scratch_shapes=[
            pltpu.VMEM((NY, 2, ROWS, 128), BF16),
            pltpu.VMEM((4, BLOCK, 128), BF16),
            pltpu.VMEM((nz, 3, ROWS, 128), BF16),
            pltpu.VMEM((384, BLOCK), F32),
            pltpu.VMEM((8, BLOCK), F32),
            pltpu.VMEM((NY, 384, ROWS), BF16),
            pltpu.VMEM((NY, 384, ROWS), BF16),
            pltpu.VMEM((NY, 8, ROWS), F32),
            pltpu.VMEM((NY, NX, 192, ROWS), BF16),
            pltpu.VMEM((BLOCK, 768), BF16),
            pltpu.VMEM((768, D), BF16),
            pltpu.VMEM((BLOCK, D), BF16),
            pltpu.VMEM((nz * ROWS, FB), BF16),
            pltpu.VMEM((nz * ROWS, FB), BF16),
            pltpu.VMEM((NB, BLOCK, FB), BF16),
            pltpu.VMEM((NB, BLOCK, FB), BF16),
            pltpu.VMEM((BLOCK, D), BF16),
            pltpu.VMEM((BLOCK, D), BF16),
            pltpu.VMEM((NB, 2, BLOCK // 2, FB), BF16),
            pltpu.VMEM((NB, BLOCK // 2, FB), BF16),
            pltpu.VMEM((16, 16, D), BF16),
            pltpu.VMEM((16, 16, D), BF16),
            dma(5),
            dma(3),
            dma(3),
            dma(2, half, 3),
            dma(2, half, 3),
            dma(3, 2),
            dma(3, 2),
            dma(2, half, 2),
            dma(2, half, 2),
            dma(3),
            dma(3),
            dma(3, 2),
            dma(3, 2),
            dma(3, 2),
            dma(3, 2),
            dma(15),
            dma(15),
            dma(NB),
            dma(NB),
            dma(NB),
            dma(NB),
            dma(15),
            dma(15),
            dma(3),
            dma(3),
            dma(4),
            dma(4),
        ],
        compiler_params=pltpu.CompilerParams(
            collective_id=0, has_side_effects=True, vmem_limit_bytes=60 * 1024 * 1024
        ),
    )(
        qkv,
        balances,
        gains,
        mlp_gain.reshape(1, D),
        residual,
        out_first,
        out_second,
        up_weight,
        down_weight,
    )


def solution(mesh):
    heads = P("sp", "tp", None)
    whole = P("sp", "tp")
    in_specs = (
        P("sp", None),
        *([heads] * 6),
        P("tp"),
        P("tp"),
        P(),
        P(),
        P("tp", None),
        P("tp", None),
        P(),
        whole,
        whole,
    )
    return jax.shard_map(
        layer, mesh=mesh, in_specs=in_specs, out_specs=P("sp", None), check_vma=False
    )
```

time: 379 us -> 123 us (0.32)
  waiting for transfers between devices: 272 us -> 0 us
  Pallas kernels: 0 us -> 112 us
  blocking collectives: 62.9 us -> 0 us
  between operations: 13.3 us -> 1.35 us
  matrix products: 11 us -> 0 us
  other arithmetic: 8.65 us -> 1.35 us
    all_gather x3 -> x0, waiting for transfers between devices: 272 us -> none  [the longest x2 230 us: side_by_side(): lax.all_gather(both, axis, axis=dim, tiled=True)]
    pallas_call x0 -> x1, Pallas kernels: none -> 112 us  [layer(): pl.pallas_call(functools.partial(kernel, nz), out_shape=jax.ShapeDtypeStr...]
    all_to_all x1 -> x0, blocking collectives: 62.9 us -> none  [copy_for_each(): lax.all_to_all(jnp.broadcast_to(value[None], (length, *value.shape)), axi...]
    dot_general x9 -> x0, matrix products: 11 us -> none  [the longest x1 6.39 us: body(): lax.dot_general(hidden, down_whole, (((1,), (1,)), ((), ())), preferred_e...]
    split x2 -> x0, local copies, waits for them, and re-layouts: 5.59 us -> none  [side_by_side(): jnp.split(lax.all_gather(both, axis, axis=dim, tiled=True), ends, axis=al...]
    reduce_sum x7 -> x0, other arithmetic: 4.19 us -> none  [the longest x1 3 us: over_pieces(): return tiles.sum(axis=0)]
    unnamed x17 -> x24, local copies, waits for them, and re-layouts: 3.01 us -> 7.02 us
  transfers between devices with their start and end apart: 3 -> 0, of which waited for: 3 -> 0; matrix products, arithmetic and copies ran while one was open for 4% -> 0% of each run, Pallas kernels for 0% -> 0%
where the time goes in v1:
time: 123 us; the launch traced here: 122 us
  Pallas kernels  112 us (91%)
  local copies, waits for them, and re-layouts  7.02 us (6%)
  other arithmetic  1.35 us (1%)
  between operations  1.35 us (1%)
    pallas_call x1, Pallas kernels, layer(): pl.pallas_call(functools.partial(kernel, nz), out_shape=jax.ShapeDtypeStr...  112 us
    unnamed x24, local copies, waits for them, and re-layouts  7.02 us

profile of v1, /device:TPU:1, one launch (start us, length us, event | category | flops | bytes accessed | tf_op | source)
XLA Modules:
  0.0 121.7 jit_solution(8903461145454947362)
XLA Ops:
  1.3 0.6 pad_maximum_fusion.1.balances
  1.9 0.0 copy-start.7
  1.9 0.7 copy-done.7
  2.6 0.0 copy-start.6
  2.6 0.1 maximum_bitcast_fusion.1
  2.7 0.6 copy-done.6
  3.2 0.5 pad_maximum_fusion.gains
  3.8 0.0 copy-start.4
  3.8 0.8 copy.17
  4.6 0.0 copy-done.4
  4.6 0.0 copy-start.5
  4.7 0.1 copy.18
  4.8 0.0 copy-start.1
  4.8 0.6 copy-done.5
  5.4 0.1 copy.19
  5.5 0.1 copy-done.1
  5.5 0.0 copy-start.2
  5.6 0.7 copy-done.2
  6.3 0.0 copy-start.3
  6.3 0.7 copy-done.3
  7.1 0.1 fusion.qkv
  7.2 0.0 copy-start
  7.2 0.7 copy-done
  7.8 112.0 %shard_map.154 = bf16[128,2048]{1,0:T(8,128)(2,1)} custom-call(bf16[5,128,128]{2,1,0:T(8,128)(2,1)} %copy-done, f32[2]{0:T(128)} %pad_maximum_fusion.1.balances, f32[2,128]{1,0:T(2,128)} %pad_maximum_fusion.gains, f32[1,2048]{1,0:T(1,128)} %bitcast.22, bf16[128,2048]{1,0:T(8,128)(2,1)} %residual.1, bf16[128,2048]{1,0:T(8,128)(2,1)} %out_first.1, ...), custom_call_target="tpu_custom_call" | custom-call | tf_op jit(solution)/shard_map/pallas_call | solution.py:483
  119.9 1.9 %copy.27 = bf16[128,2048]{1,0:T(8,128)(2,1)} copy(bf16[128,2048]{1,0:T(8,128)(2,1)} %shard_map.154) | data formatting | bytes 1048576
  (4 shorter events, 0.0 us)
Async XLA Ops:
  1.9 0.7 copy-start.7
  2.6 0.7 copy-start.6
  3.8 0.8 copy-start.4
  4.6 0.7 copy-start.5
  4.8 0.8 copy-start.1
  5.5 0.8 copy-start.2
  6.3 0.8 copy-start.3
  7.2 0.7 copy-start

commit v2 on v1

v2 whole, which is shorter than its diff:
```python
import functools
import math

import jax
import jax.numpy as jnp
from jax import lax
from jax.experimental import pallas as pl
from jax.experimental.pallas import tpu as pltpu
from jax.sharding import PartitionSpec as P

MESH = pl.DeviceIdType.MESH
DK_A = 64
DK_B = 32
EPSILON = 1e-06
HEAD_SCALE = 0.8
NY = 4
NX = 4
ROWS = 128
BLOCK = NY * ROWS
D = 2048
FB = 256
NB = D // FB
LOW = -1e30
EARLY = 5
TURNS = (2, 3)
RATES = tuple(k**-0.5 * math.log2(math.e) for k in (DK_A, DK_A, DK_B, DK_B))
SPANS = ((0, 128), (128, 256), (256, 320), (320, 384))
F32 = jnp.float32
BF16 = jnp.bfloat16


def nt(a, b):
    return lax.dot_general(a, b, (((1,), (1,)), ((), ())), preferred_element_type=F32)


def kernel(
    nz,
    balance_a,
    balance_b,
    query_a,
    key_a,
    value_a,
    query_b,
    key_b,
    value_b,
    gain_a,
    gain_b,
    mlp_gain,
    residual,
    out_first,
    out_second,
    up,
    down,
    out,
    qa,
    qb,
    vraw,
    ga,
    gbb,
    bal,
    mgain,
    qpad,
    kv,
    acc,
    stats,
    xsnd,
    xacc,
    xstats,
    hx,
    hmat,
    wo,
    res,
    wup,
    wdn,
    pb,
    rb,
    mx,
    gb,
    db,
    rd,
    sb,
    rs,
    loc,
    qs,
    qr,
    ks,
    kr,
    ys,
    yr,
    ws,
    wr,
    vs,
    vr,
    os,
    orr,
    xs,
    xr,
    hs,
    hr,
    ps,
    pr,
    dsm,
    drm,
    ss,
    sr,
    fs,
    fr,
    gs,
    gr,
):
    sp = lax.axis_index("sp")
    tp = lax.axis_index("tp")
    z, y = sp // NY, sp % NY
    x, c = tp // 2, tp % 2

    def near(dy, dx):
        return (z * NY + (y + dy) % NY, ((x + dx) % NX) * 2 + c)

    partner = (sp, x * 2 + (1 - c))
    above = (((z + 1) % nz) * NY + y, tp)
    below = (((z + nz - 1) % nz) * NY + y, tp)
    others = [(dy, dx) for dy in range(NY) for dx in range(NX) if dy or dx]

    def send(src, dst, ssem, rsem, device):
        return pltpu.make_async_remote_copy(
            src_ref=src,
            dst_ref=dst,
            send_sem=ssem,
            recv_sem=rsem,
            device_id=device,
            device_id_type=MESH,
        )

    def arrive(ref, ssem, rsem):
        send(ref, ref, ssem, rsem, partner).wait_recv()

    def left(ref, ssem, rsem):
        send(ref, ref, ssem, rsem, partner).wait_send()

    barrier = pltpu.get_barrier_semaphore()
    for device in [near(dy, dx) for dy, dx in others] + [partner, above, below]:
        pl.semaphore_signal(barrier, inc=1, device_id=device, device_id_type=MESH)

    fetch = [
        pltpu.make_async_copy(value_a, vraw, loc.at[5]),
        pltpu.make_async_copy(key_a, kv.at[z, 0], loc.at[6]),
        pltpu.make_async_copy(key_b, kv.at[z, 2, pl.ds(0, 64)], loc.at[7]),
        pltpu.make_async_copy(value_b, kv.at[z, 2, pl.ds(64, 64)], loc.at[8]),
        pltpu.make_async_copy(query_a, qa.at[y], loc.at[9]),
        pltpu.make_async_copy(query_b, qb.at[y], loc.at[10]),
    ]
    for copy in fetch:
        copy.start()
    fetch[0].wait()
    kv[z, 1] = vraw[...].astype(F32).T.astype(BF16)
    for copy in fetch[1:]:
        copy.wait()
    pl.semaphore_wait(barrier, len(others) + 3)

    for ch in range(3):
        for way, device in ((0, above), (1, below)):
            send(
                kv.at[z, ch], kv.at[z, ch], ks.at[way, 0, ch], kr.at[way, 0, ch], device
            ).start()
    for d in range(1, NY):
        send(qa.at[y], qa.at[y], qs.at[d - 1, 0], qr.at[d - 1, 0], near(d, 0)).start()
        send(qb.at[y], qb.at[y], qs.at[d - 1, 1], qr.at[d - 1, 1], near(d, 0)).start()

    own = pl.ds(pl.multiple_of(z * ROWS + y * 32, 32), 32)
    mine = pl.ds(pl.multiple_of(y * FB, FB), FB)
    tok = pl.ds(pl.multiple_of(y * ROWS, ROWS), ROWS)
    side_cols = pl.ds(pl.multiple_of(c * (D // 2), D // 2), D // 2)
    ra = pl.ds(pl.multiple_of(x * 128, 128), 128)
    rbw = pl.ds(pl.multiple_of(512 + x * 64, 64), 64)
    locals_ = [
        pltpu.make_async_copy(up.at[:, mine], wup.at[own], loc.at[0]),
        pltpu.make_async_copy(down.at[:, mine], wdn.at[own], loc.at[1]),
        pltpu.make_async_copy(residual.at[:, side_cols], res.at[tok], loc.at[2]),
        pltpu.make_async_copy(out_first, wo.at[ra], loc.at[3]),
        pltpu.make_async_copy(out_second, wo.at[rbw], loc.at[4]),
        pltpu.make_async_copy(gain_a, ga, loc.at[11]),
        pltpu.make_async_copy(gain_b, gbb, loc.at[12]),
        pltpu.make_async_copy(mlp_gain, mgain, loc.at[13]),
        pltpu.make_async_copy(balance_a, bal.at[0], loc.at[14]),
        pltpu.make_async_copy(balance_b, bal.at[1], loc.at[15]),
    ]
    for copy in locals_:
        copy.start()
    for d in range(1, NX):
        send(out_first, wo.at[ra], os.at[d - 1, 0], orr.at[d - 1, 0], near(0, d)).start()
        send(out_second, wo.at[rbw], os.at[d - 1, 1], orr.at[d - 1, 1], near(0, d)).start()

    stats[pl.ds(0, 4)] = jnp.full((4, BLOCK), LOW, F32)
    stats[pl.ds(4, 4)] = jnp.zeros((4, BLOCK), F32)
    acc[...] = jnp.zeros_like(acc)

    half = nz // 2

    def step(k, ch):
        upper = lax.rem(z - (k + 1) + nz, nz)
        lower = lax.rem(z + k + 1, nz)
        ref = kv.at[upper, ch]
        arrive(ref, ks.at[0, k, ch], kr.at[0, k, ch])

        @pl.when(k < half - 1)
        def _():
            send(ref, ref, ks.at[0, k + 1, ch], kr.at[0, k + 1, ch], above).start()
            arrive(kv.at[lower, ch], ks.at[1, k, ch], kr.at[1, k, ch])

        @pl.when(k < half - 2)
        def _():
            low = kv.at[lower, ch]
            send(low, low, ks.at[1, k + 1, ch], kr.at[1, k + 1, ch], below).start()

    def join(parts, axis):
        return parts[0] if len(parts) == 1 else jnp.concatenate(parts, axis=axis)

    def attend(slots, masked):
        keys = (
            join([kv[u, 0] for u in slots], 0),
            join([kv[u, 2].astype(F32).T.astype(BF16) for u in slots], 0),
        )
        values = (
            join([kv[u, 1] for u in slots], 1),
            join([kv[u, 2, pl.ds(64, 64)] for u in slots], 1),
        )
        items = [(i, part) for i in range(4) for part in range(2)]

        def score(i, part):
            return nt(keys[i // 2], qpad[i, pl.ds(part * 256, 256)])

        ahead = [score(*item) for item in items[:2]]
        for t, (i, part) in enumerate(items):
            if t + 2 < len(items):
                ahead.append(score(*items[t + 2]))
            s = ahead[t]
            cols = pl.ds(part * 256, 256)
            lo, hi = SPANS[i]
            if masked:
                kpos = y * ROWS + lax.broadcasted_iota(jnp.int32, s.shape, 0)
                qpos = part * 256 + lax.broadcasted_iota(jnp.int32, s.shape, 1)
                visible = kpos <= qpos
                s = jnp.where(visible, s, LOW)
            old = stats[pl.ds(i, 1), cols]
            new = jnp.maximum(old, jnp.max(s, axis=0, keepdims=True))
            p = jnp.exp2((s - new) * RATES[i])
            if masked:
                p = jnp.where(visible, p, 0.0)
            alpha = jnp.exp2((old - new) * RATES[i])
            stats[pl.ds(i, 1), cols] = new
            stats[pl.ds(4 + i, 1), cols] = stats[pl.ds(4 + i, 1), cols] * alpha + jnp.sum(
                p, axis=0, keepdims=True
            )
            rows = pl.ds(lo, hi - lo)
            acc[rows, cols] = acc[rows, cols] * alpha + jnp.dot(
                values[i // 2], p.astype(BF16), preferred_element_type=F32
            )

    def sides(k):
        upper = lax.rem(z - (k + 1) + nz, nz)
        lower = lax.rem(z + k + 1, nz)
        first = k + 1 <= z
        second = (z + k + 1 >= nz) & (k < half - 1)

        @pl.when(first & second)
        def _():
            attend((upper, lower), False)

        @pl.when(first != second)
        def _():
            attend((jnp.where(first, upper, lower),), False)

    order = (0, 2, 1)
    for ch in order:
        step(0, ch)
    for d in range(1, NY):
        there = (y + NY - d) % NY
        arrive(qa.at[there], qs.at[d - 1, 0], qr.at[d - 1, 0])
        arrive(qb.at[there], qs.at[d - 1, 1], qr.at[d - 1, 1])
    for d in range(1, NY):
        part = pl.ds(pl.multiple_of(((y + d) % NY) * FB, FB), FB)
        send(up.at[:, part], wup.at[own], ys.at[d - 1, 0], yr.at[d - 1, 0], near(d, 0)).start()
        send(down.at[:, part], wdn.at[own], ys.at[d - 1, 1], yr.at[d - 1, 1], near(d, 0)).start()
    for d in range(1, NY):
        send(
            residual.at[:, side_cols], res.at[tok], vs.at[d - 1], vr.at[d - 1], near(d, 0)
        ).start()
    lane = lax.broadcasted_iota(jnp.int32, (ROWS, 128), 1)
    bounds = ((0, 64), (64, 128), (0, 32), (32, 64))
    for j in range(NY):
        rows = pl.ds(j * ROWS, ROWS)
        low = jnp.concatenate([qb[j], qb[j]], axis=0).astype(F32).T
        for i, (start, stop) in enumerate(bounds):
            keep = (lane >= start) & (lane < stop)
            whole = qa[j].astype(F32) if i < 2 else low
            qpad[i, rows] = jnp.where(keep, whole, 0.0).astype(BF16)

    for ch in order:
        step(1, ch)
    attend((z,), True)

    def shard(ref, at, i):
        return ref.at[pl.ds(pl.multiple_of(at * ROWS + (i % 2) * 64, 64), 64)]

    weights = (wup, wup, wdn, wdn)

    def ring(k, _):
        for ch in order:
            step(k, ch)
        sides(k - 2)
        return 0

    lax.fori_loop(2, EARLY, ring, 0)
    for copy in locals_:
        copy.wait()
    for d in range(1, NY):
        rows = pl.ds(pl.multiple_of(z * ROWS + ((y + NY - d) % NY) * 32, 32), 32)
        for i, w in enumerate((wup, wdn)):
            arrive(w.at[rows], ys.at[d - 1, i], yr.at[d - 1, i])
    for i, w in enumerate(weights):
        for way, device in ((0, above), (1, below)):
            ref = shard(w, z, i)
            send(ref, ref, ws.at[way, 0, i], wr.at[way, 0, i], device).start()
    lax.fori_loop(EARLY, half, ring, 0)

    def rest(k, _):
        sides(k)
        return 0

    lax.fori_loop(half - 2, half, rest, 0)

    def turn(k):
        upper = lax.rem(z - (k + 1) + nz, nz)
        lower = lax.rem(z + k + 1, nz)
        for i, w in enumerate(weights):
            ref = shard(w, upper, i)
            arrive(ref, ws.at[0, k, i], wr.at[0, k, i])
            if k < nz // 2 - 1:
                send(ref, ref, ws.at[0, k + 1, i], wr.at[0, k + 1, i], above).start()
                ref = shard(w, lower, i)
                arrive(ref, ws.at[1, k, i], wr.at[1, k, i])
                if k < nz // 2 - 2:
                    send(ref, ref, ws.at[1, k + 1, i], wr.at[1, k + 1, i], below).start()

    turns = list(range(nz // 2))

    def turn_some(count):
        for k in turns[:count]:
            turn(k)
        del turns[:count]

    for j in range(NY):
        xsnd[j] = acc[:, pl.ds(j * ROWS, ROWS)].astype(BF16)
    for d in range(1, NY):
        there = (y + d) % NY
        part = stats.at[:, pl.ds(pl.multiple_of(there * ROWS, ROWS), ROWS)]
        send(xsnd.at[there], xacc.at[y], xs.at[d - 1, 0], xr.at[d - 1, 0], near(d, 0)).start()
        send(part, xstats.at[y], xs.at[d - 1, 1], xr.at[d - 1, 1], near(d, 0)).start()
    xacc[y] = xsnd[y]
    xstats[y] = stats[:, tok]
    turn_some(TURNS[0])
    for d in range(1, NY):
        there = (y + NY - d) % NY
        arrive(xacc.at[there], xs.at[d - 1, 0], xr.at[d - 1, 0])
        arrive(xstats.at[there], xs.at[d - 1, 1], xr.at[d - 1, 1])

    maps = []
    for i in range(4):
        lo, hi = SPANS[i]
        tops = [xstats[j, i : i + 1] for j in range(NY)]
        top = functools.reduce(jnp.maximum, tops)
        shares = [jnp.exp2((t - top) * RATES[i]) for t in tops]
        total = sum(w * xstats[j, 4 + i : 5 + i] for j, w in enumerate(shares))
        maps.append(
            sum(
                xacc[j, pl.ds(lo, hi - lo)].astype(F32) * (w / total)
                for j, w in enumerate(shares)
            )
        )
    for g in range(2):
        mixed = maps[2 * g] - bal[g, 0] * maps[2 * g + 1]
        size = mixed.shape[0]
        power = jnp.mean(mixed * mixed, axis=0, keepdims=True)
        gain = jnp.broadcast_to((ga, gbb)[g][...], (128, size)).T
        normed = mixed * lax.rsqrt(power + EPSILON) * gain * HEAD_SCALE
        hx[y, x, pl.ds(128 * g, size)] = normed.astype(BF16)
    for n, (dy, dx) in enumerate(others):
        send(hx.at[y, x], hx.at[y, x], hs.at[n], hr.at[n], near(dy, dx)).start()
    turn_some(TURNS[1])
    for d in range(1, NX):
        there = (x + NX - d) % NX
        for i, (size, base) in enumerate(((128, 0), (64, 512))):
            ref = wo.at[pl.ds(pl.multiple_of(base + there * size, size), size)]
            arrive(ref, os.at[d - 1, i], orr.at[d - 1, i])
    for n, (dy, dx) in enumerate(others):
        ref = hx.at[(y + NY - dy) % NY, (x + NX - dx) % NX]
        arrive(ref, hs.at[n], hr.at[n])
    turn_some(1)
    for j in range(NY):
        rows = pl.ds(j * ROWS, ROWS)
        for i in range(NX):
            hmat[rows, pl.ds(i * 128, 128)] = hx[j, i, pl.ds(0, 128)].astype(F32).T.astype(BF16)
        for i in range(NX // 2):
            pair = jnp.concatenate(
                [hx[j, 2 * i, pl.ds(128, 64)], hx[j, 2 * i + 1, pl.ds(128, 64)]], axis=0
            )
            hmat[rows, pl.ds(512 + i * 128, 128)] = pair.astype(F32).T.astype(BF16)

    def block(n):
        return pl.ds(pl.multiple_of(n * FB, FB), FB)

    def project(n, _):
        p = jnp.dot(hmat[...], wo[:, block(n)], preferred_element_type=F32)
        pb[n] = p.astype(BF16)
        send(pb.at[n], rb.at[n], ps.at[n], pr.at[n], partner).start()
        return 0

    def project_own(i, _):
        n = c * (NB // 2) + i
        p = jnp.dot(hmat[...], wo[:, block(n)], preferred_element_type=F32)
        pb[n] = (p + res[:, block(i)].astype(F32)).astype(BF16)
        send(pb.at[n], rb.at[n], ps.at[n], pr.at[n], partner).start()
        return 0

    other = (1 - c) * (NB // 2)
    lax.fori_loop(other, other + NB // 2, project, 0)
    for d in range(1, NY):
        there = pl.ds(pl.multiple_of(((y + NY - d) % NY) * ROWS, ROWS), ROWS)
        arrive(res.at[there], vs.at[d - 1], vr.at[d - 1])
    lax.fori_loop(0, NB // 2, project_own, 0)
    turn_some(1)

    def mix(n, power):
        arrive(rb.at[n], ps.at[n], pr.at[n])
        cols = block(n)
        mixed = (pb[n].astype(F32) + rb[n].astype(F32)).astype(BF16)
        mx[:, cols] = mixed
        wide = mixed.astype(F32)
        gb[:, cols] = (wide * mgain[:, cols]).astype(BF16)
        square = wide * wide
        return power + (square[:, 0:128] + square[:, 128:256])

    power = lax.fori_loop(0, NB, mix, jnp.zeros((BLOCK, 128), F32))
    scale = lax.rsqrt(jnp.sum(power, axis=-1, keepdims=True) * (1.0 / D) + EPSILON)
    turn_some(len(turns))
    lifted = jnp.dot(gb[...], wup[...], preferred_element_type=F32) * scale
    active = jnp.maximum(lifted, 0.0)
    gb[:, pl.ds(0, FB)] = (active * active).astype(BF16)

    def lower_part(n, _):
        rows = pl.ds(pl.multiple_of(n * FB, FB), FB)
        term = nt(gb[:, pl.ds(0, FB)], wdn[rows]).astype(BF16)
        for j in range(NY):
            for h in range(2):
                at = j * ROWS + h * 64
                db[n, h, pl.ds(j * 64, 64)] = term[at : at + 64]
        send(db.at[n, 1 - c], rd.at[n], dsm.at[n], drm.at[n], partner).start()
        return 0

    def gather(n, _):
        arrive(rd.at[n], dsm.at[n], drm.at[n])
        both = (db[n, c].astype(F32) + rd[n].astype(F32)).astype(BF16)
        cols = pl.ds(pl.multiple_of((n % (NB // 2)) * FB, FB), FB)
        for j in range(16):
            sb[n // (NB // 2), j, :, cols] = both[j * 16 : j * 16 + 16]
        return 0

    here = y * NX + x

    def scatter(h):
        for n, (dy, dx) in enumerate(others):
            to = ((y + dy) % NY) * NX + (x + dx) % NX
            send(sb.at[h, to], rs.at[h, here], ss.at[h, n], sr.at[h, n], near(dy, dx)).start()
        rs[h, here] = sb[h, here]

    lax.fori_loop(0, NB - 2, lower_part, 0)
    lax.fori_loop(0, NB // 2, gather, 0)
    scatter(0)
    lax.fori_loop(NB - 2, NB, lower_part, 0)
    lax.fori_loop(NB // 2, NB, gather, 0)
    scatter(1)

    def piece(core, at, h):
        rows = pl.ds(pl.multiple_of(core * 64 + at * 16, 16), 16)
        return out.at[rows, pl.ds(h * (D // 2), D // 2)]

    for h in range(2):
        for n, (dy, dx) in enumerate(others):
            ref = rs.at[h, ((y + NY - dy) % NY) * NX + (x + NX - dx) % NX]
            arrive(ref, ss.at[h, n], sr.at[h, n])

        def final(n, _):
            cols = block(n)
            added = rs[h, :, :, cols].astype(F32).sum(axis=0)
            wide = block(h * (NB // 2) + n)
            base = mx[pl.ds(pl.multiple_of(y * ROWS + c * 64 + x * 16, 16), 16), wide]
            total = (base.astype(F32) + added).astype(BF16)
            out[pl.ds(pl.multiple_of(c * 64 + x * 16, 16), 16), wide] = total
            return 0

        lax.fori_loop(0, NB // 2, final, 0)
        ref = piece(c, x, h)
        for d in range(1, NX):
            send(ref, ref, fs.at[h, d - 1], fr.at[h, d - 1], near(0, d)).start()
        send(ref, ref, gs.at[h, 0], gr.at[h, 0], partner).start()
    for h in range(2):
        for d in range(1, NX):
            ref = piece(c, (x + NX - d) % NX, h)
            arrive(ref, fs.at[h, d - 1], fr.at[h, d - 1])
            send(ref, ref, gs.at[h, d], gr.at[h, d], partner).start()
    for h in range(2):
        for d in range(NX):
            arrive(piece(1 - c, (x + NX - d) % NX, h), gs.at[h, d], gr.at[h, d])

    for d in range(NX - 1):
        for h in range(2):
            left(piece(c, x, h), fs.at[h, d], fr.at[h, d])
        left(out_first, os.at[d, 0], orr.at[d, 0])
        left(out_second, os.at[d, 1], orr.at[d, 1])
    for d in range(NX):
        for h in range(2):
            left(piece(c, x, h), gs.at[h, d], gr.at[h, d])
    for d in range(NY - 1):
        left(qa.at[0], qs.at[d, 0], qr.at[d, 0])
        left(qb.at[0], qs.at[d, 1], qr.at[d, 1])
        left(up.at[:, mine], ys.at[d, 0], yr.at[d, 0])
        left(down.at[:, mine], ys.at[d, 1], yr.at[d, 1])
        left(res.at[tok], vs.at[d], vr.at[d])
        left(xsnd.at[0], xs.at[d, 0], xr.at[d, 0])
        left(xstats.at[0], xs.at[d, 1], xr.at[d, 1])
    for n in range(len(others)):
        left(hx.at[0, 0], hs.at[n], hr.at[n])
        for h in range(2):
            left(sb.at[h, 0], ss.at[h, n], sr.at[h, n])
    for n in range(NB):
        left(pb.at[0], ps.at[n], pr.at[n])
        left(rd.at[0], dsm.at[n], drm.at[n])
    for way, steps in ((0, nz // 2), (1, nz // 2 - 1)):
        for k in range(steps):
            for ch in range(3):
                left(kv.at[0, ch], ks.at[way, k, ch], kr.at[way, k, ch])
            for i in range(4):
                left(shard(wup, 0, 0), ws.at[way, k, i], wr.at[way, k, i])


def layer(
    residual,
    query_first,
    key_first,
    value_first,
    query_second,
    key_second,
    value_second,
    balance_first,
    balance_second,
    head_gain_first,
    head_gain_second,
    out_first,
    out_second,
    mlp_gain,
    up_weight,
    down_weight,
):
    nz = lax.axis_size("sp") // NY
    flat = lambda a: a.reshape(a.shape[0], a.shape[2])
    vmem = pl.BlockSpec(memory_space=pltpu.VMEM)
    anywhere = pl.BlockSpec(memory_space=pl.ANY)
    half = nz // 2
    dma = lambda *shape: pltpu.SemaphoreType.DMA(shape)
    return pl.pallas_call(
        functools.partial(kernel, nz),
        out_shape=jax.ShapeDtypeStruct((ROWS, D), BF16),
        in_specs=[anywhere] * 16,
        out_specs=vmem,
        scratch_shapes=[
            pltpu.VMEM((NY, ROWS, 128), BF16),
            pltpu.VMEM((NY, 64, 128), BF16),
            pltpu.VMEM((ROWS, 128), BF16),
            pltpu.VMEM((1, 128), F32),
            pltpu.VMEM((1, 64), F32),
            pltpu.SMEM((2, 1), F32),
            pltpu.VMEM((1, D), F32),
            pltpu.VMEM((4, BLOCK, 128), BF16),
            pltpu.VMEM((nz, 3, ROWS, 128), BF16),
            pltpu.VMEM((384, BLOCK), F32),
            pltpu.VMEM((8, BLOCK), F32),
            pltpu.VMEM((NY, 384, ROWS), BF16),
            pltpu.VMEM((NY, 384, ROWS), BF16),
            pltpu.VMEM((NY, 8, ROWS), F32),
            pltpu.VMEM((NY, NX, 192, ROWS), BF16),
            pltpu.VMEM((BLOCK, 768), BF16),
            pltpu.VMEM((768, D), BF16),
            pltpu.VMEM((BLOCK, D // 2), BF16),
            pltpu.VMEM((nz * ROWS, FB), BF16),
            pltpu.VMEM((nz * ROWS, FB), BF16),
            pltpu.VMEM((NB, BLOCK, FB), BF16),
            pltpu.VMEM((NB, BLOCK, FB), BF16),
            pltpu.VMEM((BLOCK, D), BF16),
            pltpu.VMEM((BLOCK, D), BF16),
            pltpu.VMEM((NB, 2, BLOCK // 2, FB), BF16),
            pltpu.VMEM((NB, BLOCK // 2, FB), BF16),
            pltpu.VMEM((2, 16, 16, D // 2), BF16),
            pltpu.VMEM((2, 16, 16, D // 2), BF16),
            dma(16),
            dma(3, 2),
            dma(3, 2),
            dma(2, half, 3),
            dma(2, half, 3),
            dma(3, 2),
            dma(3, 2),
            dma(2, half, 4),
            dma(2, half, 4),
            dma(3),
            dma(3),
            dma(3, 2),
            dma(3, 2),
            dma(3, 2),
            dma(3, 2),
            dma(15),
            dma(15),
            dma(NB),
            dma(NB),
            dma(NB),
            dma(NB),
            dma(2, 15),
            dma(2, 15),
            dma(2, 3),
            dma(2, 3),
            dma(2, 4),
            dma(2, 4),
        ],
        compiler_params=pltpu.CompilerParams(
            collective_id=0, has_side_effects=True, vmem_limit_bytes=60 * 1024 * 1024
        ),
    )(
        balance_first,
        balance_second,
        flat(query_first),
        flat(key_first),
        flat(value_first),
        flat(query_second).T,
        flat(key_second).T,
        flat(value_second).T,
        head_gain_first.reshape(1, -1),
        head_gain_second.reshape(1, -1),
        mlp_gain.reshape(1, D),
        residual,
        out_first,
        out_second,
        up_weight,
        down_weight,
    )


def solution(mesh):
    heads = P("sp", "tp", None)
    whole = P("sp", "tp")
    in_specs = (
        P("sp", None),
        *([heads] * 6),
        P("tp"),
        P("tp"),
        P(),
        P(),
        P("tp", None),
        P("tp", None),
        P(),
        whole,
        whole,
    )
    return jax.shard_map(
        layer, mesh=mesh, in_specs=in_specs, out_specs=P("sp", None), check_vma=False
    )
```

time: 123 us -> 107 us (0.87); the launches traced: 122 us -> 107 us
  Pallas kernels: 112 us -> 104 us
  local copies, waits for them, and re-layouts: 7.02 us -> 1.88 us
  other arithmetic: 1.35 us -> 0 us
    pallas_call x1, Pallas kernels: 112 us -> 104 us  [layer(): pl.pallas_call(functools.partial(kernel, nz), out_shape=jax.ShapeDtypeStr...]
    unnamed x24 -> x1, local copies, waits for them, and re-layouts: 7.02 us -> 1.88 us
where the time goes in v2:
time: 107 us
  Pallas kernels  104 us (97%)
  local copies, waits for them, and re-layouts  1.88 us (2%)
  between operations  1.3 us (1%)
    pallas_call x1, Pallas kernels, layer(): pl.pallas_call(functools.partial(kernel, nz), out_shape=jax.ShapeDtypeStr...  104 us

profile of v2, /device:TPU:1, one launch (start us, length us, event | category | flops | bytes accessed | tf_op | source)
XLA Modules:
  0.0 107.2 jit_solution(7174788365218049271)
XLA Ops:
  1.3 104.0 %shard_map.154 = bf16[128,2048]{1,0:T(8,128)(2,1)} custom-call(f32[1]{0:T(128)S(6)} %copy.18.balance_a, f32[1]{0:T(128)S(6)} %copy.19.balance_b, bf16[128,128]{1,0:T(8,128)(2,1)} %bitcast.15, bf16[128,128]{1,0:T(8,128)(2,1)} %bitcast.16, bf16[128,128]{1,0:T(8,128)(2,1)} %bitcast.17, bf16[64,128]{1,0:T(8,128)(2,1)} %bitcast.18, bf16[64,128]{1,0:T(8,128)(2,1)} %bitcast.19, ...), custom_call_target="tpu_custom_call" | custom-call | tf_op jit(solution)/shard_map/pallas_call | solution.py:570
  105.3 1.9 %copy.20 = bf16[128,2048]{1,0:T(8,128)(2,1)} copy(bf16[128,2048]{1,0:T(8,128)(2,1)} %shard_map.154) | data formatting | bytes 1048576

commit v3 on v2

--- a/solution.py
+++ b/solution.py
@@ -21,8 +21,11 @@
 FB = 256
 NB = D // FB
 LOW = -1e30
-EARLY = 5
-TURNS = (2, 3)
+EARLY = 2
+TURNS = (4, 6, 0, 1)
+QN = 4
+QB = NB // QN
+QW = D // QN
 RATES = tuple(k**-0.5 * math.log2(math.e) for k in (DK_A, DK_A, DK_B, DK_B))
 SPANS = ((0, 128), (128, 256), (256, 320), (320, 384))
 F32 = jnp.float32
@@ -70,8 +73,7 @@
     hmat,
     wo,
     res,
-    wup,
-    wdn,
+    wt,
     pb,
     rb,
     mx,
@@ -160,7 +162,7 @@
     for ch in range(3):
         for way, device in ((0, above), (1, below)):
             send(
-                kv.at[z, ch], kv.at[z, ch], ks.at[way, 0, ch], kr.at[way, 0, ch], device
+                kv.at[z, ch], kv.at[z, ch], ks, kr.at[way, 0, ch], device
             ).start()
     for d in range(1, NY):
         send(qa.at[y], qa.at[y], qs.at[d - 1, 0], qr.at[d - 1, 0], near(d, 0)).start()
@@ -173,8 +175,8 @@
     ra = pl.ds(pl.multiple_of(x * 128, 128), 128)
     rbw = pl.ds(pl.multiple_of(512 + x * 64, 64), 64)
     locals_ = [
-        pltpu.make_async_copy(up.at[:, mine], wup.at[own], loc.at[0]),
-        pltpu.make_async_copy(down.at[:, mine], wdn.at[own], loc.at[1]),
+        pltpu.make_async_copy(up.at[:, mine], wt.at[0, own], loc.at[0]),
+        pltpu.make_async_copy(down.at[:, mine], wt.at[1, own], loc.at[1]),
         pltpu.make_async_copy(residual.at[:, side_cols], res.at[tok], loc.at[2]),
         pltpu.make_async_copy(out_first, wo.at[ra], loc.at[3]),
         pltpu.make_async_copy(out_second, wo.at[rbw], loc.at[4]),
@@ -200,17 +202,17 @@
         upper = lax.rem(z - (k + 1) + nz, nz)
         lower = lax.rem(z + k + 1, nz)
         ref = kv.at[upper, ch]
-        arrive(ref, ks.at[0, k, ch], kr.at[0, k, ch])
+        arrive(ref, ks, kr.at[0, k, ch])
 
         @pl.when(k < half - 1)
         def _():
-            send(ref, ref, ks.at[0, k + 1, ch], kr.at[0, k + 1, ch], above).start()
-            arrive(kv.at[lower, ch], ks.at[1, k, ch], kr.at[1, k, ch])
+            send(ref, ref, ks, kr.at[0, k + 1, ch], above).start()
+            arrive(kv.at[lower, ch], ks, kr.at[1, k, ch])
 
         @pl.when(k < half - 2)
         def _():
             low = kv.at[lower, ch]
-            send(low, low, ks.at[1, k + 1, ch], kr.at[1, k + 1, ch], below).start()
+            send(low, low, ks, kr.at[1, k + 1, ch], below).start()
 
     def join(parts, axis):
         return parts[0] if len(parts) == 1 else jnp.concatenate(parts, axis=axis)
@@ -279,8 +281,8 @@
         arrive(qb.at[there], qs.at[d - 1, 1], qr.at[d - 1, 1])
     for d in range(1, NY):
         part = pl.ds(pl.multiple_of(((y + d) % NY) * FB, FB), FB)
-        send(up.at[:, part], wup.at[own], ys.at[d - 1, 0], yr.at[d - 1, 0], near(d, 0)).start()
-        send(down.at[:, part], wdn.at[own], ys.at[d - 1, 1], yr.at[d - 1, 1], near(d, 0)).start()
+        send(up.at[:, part], wt.at[0, own], ys.at[d - 1, 0], yr.at[d - 1, 0], near(d, 0)).start()
+        send(down.at[:, part], wt.at[1, own], ys.at[d - 1, 1], yr.at[d - 1, 1], near(d, 0)).start()
     for d in range(1, NY):
         send(
             residual.at[:, side_cols], res.at[tok], vs.at[d - 1], vr.at[d - 1], near(d, 0)
@@ -299,29 +301,59 @@
         step(1, ch)
     attend((z,), True)
 
-    def shard(ref, at, i):
-        return ref.at[pl.ds(pl.multiple_of(at * ROWS + (i % 2) * 64, 64), 64)]
-
-    weights = (wup, wup, wdn, wdn)
+    def shard(at, i, h):
+        return wt.at[i, pl.ds(pl.multiple_of(at * ROWS + h * 64, 64), 64)]
+
+    def half_turn(w):
+        k, i = w // 2, w % 2
+        upper = lax.rem(z - (k + 1) + nz, nz)
+        lower = lax.rem(z + k + 1, nz)
+        for h in range(2):
+            n = i * 2 + h
+            ref = shard(upper, i, h)
+            low = shard(lower, i, h)
+            arrive(ref, ws.at[i], wr.at[0, k, n])
+
+            def onward(ref=ref, low=low, n=n):
+                send(ref, ref, ws.at[i], wr.at[0, k + 1, n], above).start()
+                arrive(low, ws.at[i], wr.at[1, k, n])
+
+            def downward(low=low, n=n):
+                send(low, low, ws.at[i], wr.at[1, k + 1, n], below).start()
+
+            if isinstance(w, int):
+                if k < half - 1:
+                    onward()
+                if k < half - 2:
+                    downward()
+            else:
+                pl.when(k < half - 1)(onward)
+                pl.when(k < half - 2)(downward)
 
     def ring(k, _):
         for ch in order:
             step(k, ch)
         sides(k - 2)
+
+        @pl.when(k > EARLY)
+        def _():
+            half_turn(k - EARLY - 1)
+
         return 0
 
-    lax.fori_loop(2, EARLY, ring, 0)
     for copy in locals_:
         copy.wait()
     for d in range(1, NY):
         rows = pl.ds(pl.multiple_of(z * ROWS + ((y + NY - d) % NY) * 32, 32), 32)
-        for i, w in enumerate((wup, wdn)):
-            arrive(w.at[rows], ys.at[d - 1, i], yr.at[d - 1, i])
-    for i, w in enumerate(weights):
-        for way, device in ((0, above), (1, below)):
-            ref = shard(w, z, i)
-            send(ref, ref, ws.at[way, 0, i], wr.at[way, 0, i], device).start()
-    lax.fori_loop(EARLY, half, ring, 0)
+        for i in range(2):
+            arrive(wt.at[i, rows], ys.at[d - 1, i], yr.at[d - 1, i])
+    for i in range(2):
+        for h in range(2):
+            for way, device in ((0, above), (1, below)):
+                ref = shard(z, i, h)
+                n = i * 2 + h
+                send(ref, ref, ws.at[n // 2], wr.at[way, 0, n], device).start()
+    lax.fori_loop(2, half, ring, 0)
 
     def rest(k, _):
         sides(k)
@@ -329,24 +361,11 @@
 
     lax.fori_loop(half - 2, half, rest, 0)
 
-    def turn(k):
-        upper = lax.rem(z - (k + 1) + nz, nz)
-        lower = lax.rem(z + k + 1, nz)
-        for i, w in enumerate(weights):
-            ref = shard(w, upper, i)
-            arrive(ref, ws.at[0, k, i], wr.at[0, k, i])
-            if k < nz // 2 - 1:
-                send(ref, ref, ws.at[0, k + 1, i], wr.at[0, k + 1, i], above).start()
-                ref = shard(w, lower, i)
-                arrive(ref, ws.at[1, k, i], wr.at[1, k, i])
-                if k < nz // 2 - 2:
-                    send(ref, ref, ws.at[1, k + 1, i], wr.at[1, k + 1, i], below).start()
-
-    turns = list(range(nz // 2))
+    turns = list(range(half - EARLY - 1, 2 * half))
 
     def turn_some(count):
         for k in turns[:count]:
-            turn(k)
+            half_turn(k)
         del turns[:count]
 
     for j in range(NY):
@@ -385,17 +404,15 @@
         normed = mixed * lax.rsqrt(power + EPSILON) * gain * HEAD_SCALE
         hx[y, x, pl.ds(128 * g, size)] = normed.astype(BF16)
     for n, (dy, dx) in enumerate(others):
-        send(hx.at[y, x], hx.at[y, x], hs.at[n], hr.at[n], near(dy, dx)).start()
+        send(hx.at[y, x], hx.at[y, x], hs, hr, near(dy, dx)).start()
     turn_some(TURNS[1])
     for d in range(1, NX):
         there = (x + NX - d) % NX
         for i, (size, base) in enumerate(((128, 0), (64, 512))):
             ref = wo.at[pl.ds(pl.multiple_of(base + there * size, size), size)]
             arrive(ref, os.at[d - 1, i], orr.at[d - 1, i])
-    for n, (dy, dx) in enumerate(others):
-        ref = hx.at[(y + NY - dy) % NY, (x + NX - dx) % NX]
-        arrive(ref, hs.at[n], hr.at[n])
-    turn_some(1)
+    arrive(hmat.at[pl.ds(0, 480)], hs, hr)
+    turn_some(TURNS[2])
     for j in range(NY):
         rows = pl.ds(j * ROWS, ROWS)
         for i in range(NX):
@@ -412,14 +429,14 @@
     def project(n, _):
         p = jnp.dot(hmat[...], wo[:, block(n)], preferred_element_type=F32)
         pb[n] = p.astype(BF16)
-        send(pb.at[n], rb.at[n], ps.at[n], pr.at[n], partner).start()
+        send(pb.at[n], rb.at[n], ps, pr.at[n], partner).start()
         return 0
 
     def project_own(i, _):
         n = c * (NB // 2) + i
         p = jnp.dot(hmat[...], wo[:, block(n)], preferred_element_type=F32)
         pb[n] = (p + res[:, block(i)].astype(F32)).astype(BF16)
-        send(pb.at[n], rb.at[n], ps.at[n], pr.at[n], partner).start()
+        send(pb.at[n], rb.at[n], ps, pr.at[n], partner).start()
         return 0
 
     other = (1 - c) * (NB // 2)
@@ -428,10 +445,10 @@
         there = pl.ds(pl.multiple_of(((y + NY - d) % NY) * ROWS, ROWS), ROWS)
         arrive(res.at[there], vs.at[d - 1], vr.at[d - 1])
     lax.fori_loop(0, NB // 2, project_own, 0)
-    turn_some(1)
+    turn_some(TURNS[3])
 
     def mix(n, power):
-        arrive(rb.at[n], ps.at[n], pr.at[n])
+        arrive(rb.at[n], ps, pr.at[n])
         cols = block(n)
         mixed = (pb[n].astype(F32) + rb[n].astype(F32)).astype(BF16)
         mx[:, cols] = mixed
@@ -443,26 +460,26 @@
     power = lax.fori_loop(0, NB, mix, jnp.zeros((BLOCK, 128), F32))
     scale = lax.rsqrt(jnp.sum(power, axis=-1, keepdims=True) * (1.0 / D) + EPSILON)
     turn_some(len(turns))
-    lifted = jnp.dot(gb[...], wup[...], preferred_element_type=F32) * scale
+    lifted = jnp.dot(gb[...], wt[0], preferred_element_type=F32) * scale
     active = jnp.maximum(lifted, 0.0)
     gb[:, pl.ds(0, FB)] = (active * active).astype(BF16)
 
     def lower_part(n, _):
         rows = pl.ds(pl.multiple_of(n * FB, FB), FB)
-        term = nt(gb[:, pl.ds(0, FB)], wdn[rows]).astype(BF16)
+        term = nt(gb[:, pl.ds(0, FB)], wt[1, rows]).astype(BF16)
         for j in range(NY):
             for h in range(2):
                 at = j * ROWS + h * 64
                 db[n, h, pl.ds(j * 64, 64)] = term[at : at + 64]
-        send(db.at[n, 1 - c], rd.at[n], dsm.at[n], drm.at[n], partner).start()
+        send(db.at[n, 1 - c], rd.at[n], dsm, drm.at[n], partner).start()
         return 0
 
     def gather(n, _):
-        arrive(rd.at[n], dsm.at[n], drm.at[n])
+        arrive(rd.at[n], dsm, drm.at[n])
         both = (db[n, c].astype(F32) + rd[n].astype(F32)).astype(BF16)
-        cols = pl.ds(pl.multiple_of((n % (NB // 2)) * FB, FB), FB)
+        cols = pl.ds(pl.multiple_of((n % QB) * FB, FB), FB)
         for j in range(16):
-            sb[n // (NB // 2), j, :, cols] = both[j * 16 : j * 16 + 16]
+            sb[n // QB, j, :, cols] = both[j * 16 : j * 16 + 16]
         return 0
 
     here = y * NX + x
@@ -470,56 +487,16 @@
     def scatter(h):
         for n, (dy, dx) in enumerate(others):
             to = ((y + dy) % NY) * NX + (x + dx) % NX
-            send(sb.at[h, to], rs.at[h, here], ss.at[h, n], sr.at[h, n], near(dy, dx)).start()
+            send(sb.at[h, to], rs.at[h, here], ss, sr.at[h], near(dy, dx)).start()
         rs[h, here] = sb[h, here]
 
-    lax.fori_loop(0, NB - 2, lower_part, 0)
-    lax.fori_loop(0, NB // 2, gather, 0)
-    scatter(0)
-    lax.fori_loop(NB - 2, NB, lower_part, 0)
-    lax.fori_loop(NB // 2, NB, gather, 0)
-    scatter(1)
-
-    def piece(core, at, h):
-        rows = pl.ds(pl.multiple_of(core * 64 + at * 16, 16), 16)
-        return out.at[rows, pl.ds(h * (D // 2), D // 2)]
-
-    for h in range(2):
-        for n, (dy, dx) in enumerate(others):
-            ref = rs.at[h, ((y + NY - dy) % NY) * NX + (x + NX - dx) % NX]
-            arrive(ref, ss.at[h, n], sr.at[h, n])
-
-        def final(n, _):
-            cols = block(n)
-            added = rs[h, :, :, cols].astype(F32).sum(axis=0)
-            wide = block(h * (NB // 2) + n)
-            base = mx[pl.ds(pl.multiple_of(y * ROWS + c * 64 + x * 16, 16), 16), wide]
-            total = (base.astype(F32) + added).astype(BF16)
-            out[pl.ds(pl.multiple_of(c * 64 + x * 16, 16), 16), wide] = total
-            return 0
-
-        lax.fori_loop(0, NB // 2, final, 0)
-        ref = piece(c, x, h)
-        for d in range(1, NX):
-            send(ref, ref, fs.at[h, d - 1], fr.at[h, d - 1], near(0, d)).start()
-        send(ref, ref, gs.at[h, 0], gr.at[h, 0], partner).start()
-    for h in range(2):
-        for d in range(1, NX):
-            ref = piece(c, (x + NX - d) % NX, h)
-            arrive(ref, fs.at[h, d - 1], fr.at[h, d - 1])
-            send(ref, ref, gs.at[h, d], gr.at[h, d], partner).start()
-    for h in range(2):
-        for d in range(NX):
-            arrive(piece(1 - c, (x + NX - d) % NX, h), gs.at[h, d], gr.at[h, d])
-
-    for d in range(NX - 1):
-        for h in range(2):
-            left(piece(c, x, h), fs.at[h, d], fr.at[h, d])
-        left(out_first, os.at[d, 0], orr.at[d, 0])
-        left(out_second, os.at[d, 1], orr.at[d, 1])
-    for d in range(NX):
-        for h in range(2):
-            left(piece(c, x, h), gs.at[h, d], gr.at[h, d])
+    lax.fori_loop(0, QB, lower_part, 0)
+    for h in range(QN):
+        if h + 1 < QN:
+            lax.fori_loop((h + 1) * QB, (h + 2) * QB, lower_part, 0)
+        lax.fori_loop(h * QB, (h + 1) * QB, gather, 0)
+        scatter(h)
+
     for d in range(NY - 1):
         left(qa.at[0], qs.at[d, 0], qr.at[d, 0])
         left(qb.at[0], qs.at[d, 1], qr.at[d, 1])
@@ -528,19 +505,46 @@
         left(res.at[tok], vs.at[d], vr.at[d])
         left(xsnd.at[0], xs.at[d, 0], xr.at[d, 0])
         left(xstats.at[0], xs.at[d, 1], xr.at[d, 1])
-    for n in range(len(others)):
-        left(hx.at[0, 0], hs.at[n], hr.at[n])
-        for h in range(2):
-            left(sb.at[h, 0], ss.at[h, n], sr.at[h, n])
-    for n in range(NB):
-        left(pb.at[0], ps.at[n], pr.at[n])
-        left(rd.at[0], dsm.at[n], drm.at[n])
-    for way, steps in ((0, nz // 2), (1, nz // 2 - 1)):
-        for k in range(steps):
-            for ch in range(3):
-                left(kv.at[0, ch], ks.at[way, k, ch], kr.at[way, k, ch])
-            for i in range(4):
-                left(shard(wup, 0, 0), ws.at[way, k, i], wr.at[way, k, i])
+    left(hmat.at[pl.ds(0, 480)], hs, hr)
+    left(pb, ps, pr.at[0])
+    left(rd, dsm, drm.at[0])
+    left(kv.at[pl.ds(0, nz - 1)], ks, kr.at[0, 0, 0])
+    for i in range(2):
+        left(wt.at[i, pl.ds(0, (nz - 1) * ROWS)], ws.at[i], wr.at[0, 0, 0])
+    for d in range(NX - 1):
+        left(out_first, os.at[d, 0], orr.at[d, 0])
+        left(out_second, os.at[d, 1], orr.at[d, 1])
+
+    def piece(core, at, h):
+        rows = pl.ds(pl.multiple_of(core * 64 + at * 16, 16), 16)
+        return out.at[rows, pl.ds(h * QW, QW)]
+
+    for h in range(QN):
+        arrive(rs.at[h, pl.ds(0, 15)], ss, sr.at[h])
+
+        def final(n, _):
+            cols = block(n)
+            added = rs[h, :, :, cols].astype(F32).sum(axis=0)
+            wide = block(h * QB + n)
+            base = mx[pl.ds(pl.multiple_of(y * ROWS + c * 64 + x * 16, 16), 16), wide]
+            total = (base.astype(F32) + added).astype(BF16)
+            out[pl.ds(pl.multiple_of(c * 64 + x * 16, 16), 16), wide] = total
+            return 0
+
+        lax.fori_loop(0, QB, final, 0)
+        ref = piece(c, x, h)
+        for d in range(1, NX):
+            send(ref, ref, fs, fr.at[h], near(0, d)).start()
+        send(ref, ref, gs, gr, partner).start()
+    for h in range(QN):
+        arrive(rs.at[h, pl.ds(0, 3)], fs, fr.at[h])
+        for d in range(1, NX):
+            ref = piece(c, (x + NX - d) % NX, h)
+            send(ref, ref, gs, gr, partner).start()
+    arrive(out.at[pl.ds(0, 64)], gs, gr)
+    left(out.at[pl.ds(0, 64)], gs, gr)
+    left(out.at[pl.ds(0, 48)], fs, fr.at[0])
+    left(sb.at[:, pl.ds(0, 15)], ss, sr.at[0])
 
 
 def layer(
@@ -591,24 +595,23 @@
             pltpu.VMEM((BLOCK, 768), BF16),
             pltpu.VMEM((768, D), BF16),
             pltpu.VMEM((BLOCK, D // 2), BF16),
-            pltpu.VMEM((nz * ROWS, FB), BF16),
-            pltpu.VMEM((nz * ROWS, FB), BF16),
+            pltpu.VMEM((2, nz * ROWS, FB), BF16),
             pltpu.VMEM((NB, BLOCK, FB), BF16),
             pltpu.VMEM((NB, BLOCK, FB), BF16),
             pltpu.VMEM((BLOCK, D), BF16),
             pltpu.VMEM((BLOCK, D), BF16),
             pltpu.VMEM((NB, 2, BLOCK // 2, FB), BF16),
             pltpu.VMEM((NB, BLOCK // 2, FB), BF16),
-            pltpu.VMEM((2, 16, 16, D // 2), BF16),
-            pltpu.VMEM((2, 16, 16, D // 2), BF16),
+            pltpu.VMEM((QN, 16, 16, QW), BF16),
+            pltpu.VMEM((QN, 16, 16, QW), BF16),
             dma(16),
             dma(3, 2),
             dma(3, 2),
+            pltpu.SemaphoreType.DMA,
             dma(2, half, 3),
-            dma(2, half, 3),
-            dma(3, 2),
-            dma(3, 2),
-            dma(2, half, 4),
+            dma(3, 2),
+            dma(3, 2),
+            dma(2),
             dma(2, half, 4),
             dma(3),
             dma(3),
@@ -616,18 +619,18 @@
             dma(3, 2),
             dma(3, 2),
             dma(3, 2),
-            dma(15),
-            dma(15),
+            pltpu.SemaphoreType.DMA,
+            pltpu.SemaphoreType.DMA,
+            pltpu.SemaphoreType.DMA,
             dma(NB),
+            pltpu.SemaphoreType.DMA,
             dma(NB),
-            dma(NB),
-            dma(NB),
-            dma(2, 15),
-            dma(2, 15),
-            dma(2, 3),
-            dma(2, 3),
-            dma(2, 4),
-            dma(2, 4),
+            pltpu.SemaphoreType.DMA,
+            dma(QN),
+            pltpu.SemaphoreType.DMA,
+            dma(QN),
+            pltpu.SemaphoreType.DMA,
+            pltpu.SemaphoreType.DMA,
         ],
         compiler_params=pltpu.CompilerParams(
             collective_id=0, has_side_effects=True, vmem_limit_bytes=60 * 1024 * 1024

time: 107 us -> 101 us (0.944)
  Pallas kernels: 104 us -> 97.8 us
    pallas_call x1, Pallas kernels: 104 us -> 97.8 us  [layer(): pl.pallas_call(functools.partial(kernel, nz), out_shape=jax.ShapeDtypeStr...]
where the time goes in v3:
time: 101 us
  Pallas kernels  97.8 us (97%)
  local copies, waits for them, and re-layouts  1.88 us (2%)
  between operations  1.3 us (1%)
    pallas_call x1, Pallas kernels, layer(): pl.pallas_call(functools.partial(kernel, nz), out_shape=jax.ShapeDtypeStr...  97.8 us

profile of v3, /device:TPU:1, one launch (start us, length us, event | category | flops | bytes accessed | tf_op | source)
XLA Modules:
  0.0 101.0 jit_solution(7922342229347421616)
XLA Ops:
  1.3 97.8 %shard_map.154 = bf16[128,2048]{1,0:T(8,128)(2,1)} custom-call(f32[1]{0:T(128)S(6)} %copy.18.balance_a, f32[1]{0:T(128)S(6)} %copy.19.balance_b, bf16[128,128]{1,0:T(8,128)(2,1)} %bitcast.15, bf16[128,128]{1,0:T(8,128)(2,1)} %bitcast.16, bf16[128,128]{1,0:T(8,128)(2,1)} %bitcast.17, bf16[64,128]{1,0:T(8,128)(2,1)} %bitcast.18, bf16[64,128]{1,0:T(8,128)(2,1)} %bitcast.19, ...), custom_call_target="tpu_custom_call" | custom-call | tf_op jit(solution)/shard_map/pallas_call | solution.py:574
  99.1 1.9 %copy.20 = bf16[128,2048]{1,0:T(8,128)(2,1)} copy(bf16[128,2048]{1,0:T(8,128)(2,1)} %shard_map.154) | data formatting | bytes 1048576
